TPU v7x, 32 devices: a whole 2x2x4 slice. The times are simulated.
32 devices in a mesh: grp: 2 (over y), tp: 4 (over z), dp: 4 (over x, core).
Axes of the slice: x: 2, y: 2, z: 4, core: 2. Of those that a mesh axis runs over, the one named last changes fastest.
Arguments:
- tokens: bfloat16 [128, 4096], P('grp', 'dp'), parts along dimension 0, may hold values from -6 to 6
- norm_gain: float32 [2, 4096], P(None, 'dp'), may hold values from 0.1 to 1.9
- w_query: bfloat16 [2, 4096, 512], P(None, 'dp', 'tp'), may hold values from -0.09375 to 0.09375
- w_key: bfloat16 [2, 4096, 512], P(None, 'dp', 'tp'), may hold values from -0.09375 to 0.09375
- w_value: bfloat16 [2, 4096, 512], P(None, 'dp', 'tp'), may hold values from -0.09375 to 0.09375
- w_outgate: bfloat16 [2, 4096, 512], P(None, 'dp', 'tp'), may hold values from -0.09375 to 0.09375
- gate_weight: bfloat16 [2, 4, 384, 2], P(None, 'tp'), may hold values from -0.3125 to 0.3125
- forget_bias: float32 [2, 4], P(None, 'tp'), may hold values from -2 to 4
- w_mix: bfloat16 [2, 512, 4096], P(None, 'tp', 'dp'), may hold values from -0.25 to 0.25
- memory: float32 [2, 128, 4, 128, 128], P(None, ('grp', 'dp'), 'tp'), parts along dimension 1, may hold values from -3 to 3
- normalizer: float32 [2, 128, 4, 128], P(None, ('grp', 'dp'), 'tp'), parts along dimension 1, may hold values from -3 to 3
- stabilizer: float32 [2, 128, 4], P(None, ('grp', 'dp'), 'tp'), parts along dimension 1, may hold values from -4 to 4
Outputs:
- result: bfloat16 [128, 4096], P('grp', 'dp'), parts along dimension 0
- new_memory: float32 [2, 128, 4, 128, 128], P(None, ('grp', 'dp'), 'tp'), parts along dimension 1
- new_normalizer: float32 [2, 128, 4, 128], P(None, ('grp', 'dp'), 'tp'), parts along dimension 1
- new_stabilizer: float32 [2, 128, 4], P(None, ('grp', 'dp'), 'tp'), parts along dimension 1
There are 2 independent parts, one for each index of `grp`. A program takes and returns all parts, laid end to end along the dimension named above; an argument that names none is the same for every part. Nothing has to cross between parts.
All inputs are finite; a program needn't handle non-finite values.
Results may differ from a plain program's by a relative error of at most 0.018.
Values may be sent and summed in bfloat16 or wider, within the bound.
A program may use at most 64 MiB of HBM per device.

v0:
```python
import jax
import jax.numpy as jnp
from jax import lax
from jax.sharding import PartitionSpec as P

D = 4096
DK = 128
BLOCKS = 2
EPS = 1e-06


def shards(
    tokens,
    norm_gain,
    w_query,
    w_key,
    w_value,
    w_outgate,
    gate_weight,
    forget_bias,
    w_mix,
    memory,
    normalizer,
    stabilizer,
):
    x = tokens
    seq_own = memory.shape[1]
    heads_own = memory.shape[2]
    mems, norms, stabs = ([], [], [])
    for blk in range(BLOCKS):
        xf = x.astype(jnp.float32)
        squares = jnp.sum(xf * xf, axis=-1)
        scaled_in = (xf * norm_gain[blk]).astype(jnp.bfloat16)
        terms = tuple(
            (
                jnp.dot(scaled_in, weight[blk], preferred_element_type=jnp.float32)
                for weight in (w_query, w_key, w_value, w_outgate)
            )
        )
        totals = lax.psum(squares, "dp")
        summed = lax.psum_scatter(terms, "dp", scatter_dimension=0, tiled=True)
        own_squares = lax.dynamic_slice_in_dim(totals, lax.axis_index("dp") * seq_own, seq_own, 0)
        scale = lax.rsqrt(own_squares / D + EPS)
        projs = [
            (scale[:, None] * part)
            .astype(jnp.bfloat16)
            .astype(jnp.float32)
            .reshape(seq_own, heads_own, DK)
            for part in summed
        ]
        query, key, value, outgate = projs
        joined = jnp.concatenate([query, key, value], axis=-1)
        pre = jnp.einsum(
            "shc,hcg->shg",
            joined,
            gate_weight[blk].astype(jnp.float32),
            precision=lax.Precision.HIGHEST,
        )
        log_input = pre[..., 0]
        log_forget = jax.nn.log_sigmoid(pre[..., 1] + forget_bias[blk])
        stab = stabilizer[blk]
        new_stab = jnp.maximum(log_forget + stab, log_input)
        keep = jnp.exp(log_forget + stab - new_stab)
        admit = jnp.exp(log_input - new_stab)
        scaled_key = key * DK ** (-0.5)
        new_mem = (
            keep[..., None, None] * memory[blk]
            + admit[..., None, None] * scaled_key[..., :, None] * value[..., None, :]
        )
        new_norm = keep[..., None] * normalizer[blk] + admit[..., None] * scaled_key
        numer = jnp.einsum("shd,shde->she", query, new_mem, precision=lax.Precision.HIGHEST)
        denom = jnp.maximum(jnp.abs(jnp.sum(query * new_norm, axis=-1)), 1.0)
        readout = numer / denom[..., None]
        gated = (
            (readout * jax.nn.sigmoid(outgate))
            .reshape(seq_own, heads_own * DK)
            .astype(jnp.bfloat16)
        )
        mix_weight = w_mix[blk]
        partial_mix = jnp.dot(
            lax.all_gather(gated, "dp", axis=0, tiled=True),
            mix_weight,
            preferred_element_type=jnp.float32,
        )
        mine = lax.psum_scatter(partial_mix, "tp", scatter_dimension=0, tiled=True)
        row_count = mine.shape[0]
        own_rows = lax.dynamic_slice_in_dim(xf, lax.axis_index("tp") * row_count, row_count, 0)
        updated = (own_rows + mine).astype(jnp.bfloat16)
        x = lax.all_gather(updated, "tp", axis=0, tiled=True)
        mems.append(new_mem)
        norms.append(new_norm)
        stabs.append(new_stab)
    return (x, jnp.stack(mems, axis=0), jnp.stack(norms, axis=0), jnp.stack(stabs, axis=0))


def solution(mesh):
    in_specs = (
        P("grp", "dp"),
        P(None, "dp"),
        P(None, "dp", "tp"),
        P(None, "dp", "tp"),
        P(None, "dp", "tp"),
        P(None, "dp", "tp"),
        P(None, "tp", None, None),
        P(None, "tp"),
        P(None, "tp", "dp"),
        P(None, ("grp", "dp"), "tp", None, None),
        P(None, ("grp", "dp"), "tp", None),
        P(None, ("grp", "dp"), "tp"),
    )
    out_specs = (
        P("grp", "dp"),
        P(None, ("grp", "dp"), "tp", None, None),
        P(None, ("grp", "dp"), "tp", None),
        P(None, ("grp", "dp"), "tp"),
    )
    return jax.shard_map(shards, mesh=mesh, in_specs=in_specs, out_specs=out_specs, check_vma=False)
```

profile of v0, /device:TPU:0, one launch (start us, length us, event | category | flops | bytes accessed | tf_op | source)
XLA Modules:
  0.0 279.2 jit_solution(203216173123310671)
XLA Ops:
  7.3 0.9 fusion.116
  8.2 1.8 fusion.32
  10.1 1.8 fusion.30
  12.0 1.8 fusion.34
  13.8 1.8 fusion.28
  15.7 1.0 multiply_reduce_fusion.1
  16.8 8.4 %psum.14 = f32[64]{0:T(128)S(1)} all-reduce(f32[64]{0:T(128)S(1)} %multiply_reduce_fusion.1), channel_id=1, replica_groups=mesh['grp'=2,'tp'=4,'dp'=4] {'dp'}, use_global_device_ids=true, to_apply=%region_1.0 | all-reduce | flops 64 | bytes 512 | tf_op jit(solution)/shard_map/psum | solution.py:40
  25.1 0.6 fusion.117
  25.8 7.5 %reduce-scatter.13.cloned.1.call-done = f32[16,128]{1,0:T(8,128)} async-done(((f32[64,128]{1,0:T(8,128)}), f32[16,128]{1,0:T(8,128)}) %reduce-scatter.13.cloned.1.call-update) | async-done | bytes 8208 | tf_op jit(solution)/shard_map/reduce_scatter | solution.py:41
  33.3 22.0 %reduce-scatter.15.cloned.1.call-done = f32[16,128]{1,0:T(8,128)} async-done(((f32[64,128]{1,0:T(8,128)}), f32[16,128]{1,0:T(8,128)}) %reduce-scatter.15.cloned.1.call-update) | async-done | bytes 8208 | tf_op jit(solution)/shard_map/reduce_scatter | solution.py:41
  55.3 22.5 %reduce-scatter.11.cloned.1.call-done = f32[16,128]{1,0:T(8,128)} async-done(((f32[64,128]{1,0:T(8,128)}), f32[16,128]{1,0:T(8,128)}) %reduce-scatter.11.cloned.1.call-update) | async-done | bytes 8208 | tf_op jit(solution)/shard_map/reduce_scatter | solution.py:41
  77.8 0.8 convert_bitcast_fusion.3
  78.8 0.7 fusion.70
  79.4 0.7 fusion.108
  80.4 0.8 fusion.4
  81.1 18.6 %reduce-scatter.17.cloned.1.call-done = f32[16,128]{1,0:T(8,128)} async-done(((f32[64,128]{1,0:T(8,128)}), f32[16,128]{1,0:T(8,128)}) %reduce-scatter.17.cloned.1.call-update) | async-done | bytes 8208 | tf_op jit(solution)/shard_map/reduce_scatter | solution.py:41
  99.7 0.8 multiply_convert_fusion.15
  100.5 5.2 %all_gather.12 = bf16[64,128]{1,0:T(8,128)(2,1)S(1)} all-gather(bf16[16,128]{1,0:T(8,128)(2,1)S(1)} %multiply_convert_fusion.15), channel_id=1, replica_groups=mesh['grp'=2,'tp'=4,'dp'=4] {'dp'}, dimensions={0}, use_global_device_ids=true | all-gather | bytes 20480 | tf_op jit(solution)/shard_map/all_gather | solution.py:81
  105.7 0.9 fusion.26
  106.7 20.1 %reduce-scatter.19.cloned.1.call-done = f32[16,1024]{1,0:T(8,128)} async-done(((f32[64,1024]{1,0:T(8,128)}), f32[16,1024]{1,0:T(8,128)}) %reduce-scatter.19.cloned.1.call-update) | async-done | bytes 65552 | tf_op jit(solution)/shard_map/reduce_scatter | solution.py:85
  126.8 0.8 add_convert_fusion.1
  127.6 13.4 %all_gather.13 = bf16[64,1024]{1,0:T(8,128)(2,1)S(1)} all-gather(bf16[16,1024]{1,0:T(8,128)(2,1)S(1)} %add_convert_fusion.1), channel_id=1, replica_groups=mesh['grp'=2,'tp'=4,'dp'=4] {'tp'}, dimensions={0}, use_global_device_ids=true | all-gather | bytes 163840 | tf_op jit(solution)/shard_map/all_gather | solution.py:89
  141.0 1.7 fusion.22
  142.7 1.7 fusion.20
  144.5 1.7 fusion.18
  146.3 1.7 fusion.24
  148.2 5.7 %psum.15 = f32[64]{0:T(128)S(1)} all-reduce(f32[64]{0:T(128)S(1)} %multiply_reduce_fusion), channel_id=1, replica_groups=mesh['grp'=2,'tp'=4,'dp'=4] {'dp'}, use_global_device_ids=true, to_apply=%region_9.10 | all-reduce | flops 64 | bytes 512 | tf_op jit(solution)/shard_map/psum | solution.py:40
  154.1 0.6 reduce-scatter.27.cloned.1.call-update
  154.7 9.3 %reduce-scatter.23.cloned.1.call-done = f32[16,128]{1,0:T(8,128)} async-done(((f32[64,128]{1,0:T(8,128)}), f32[16,128]{1,0:T(8,128)}) %reduce-scatter.23.cloned.1.call-update) | async-done | bytes 8208 | tf_op jit(solution)/shard_map/reduce_scatter | solution.py:41
  164.0 22.0 %reduce-scatter.25.cloned.1.call-done = f32[16,128]{1,0:T(8,128)} async-done(((f32[64,128]{1,0:T(8,128)}), f32[16,128]{1,0:T(8,128)}) %reduce-scatter.25.cloned.1.call-update) | async-done | bytes 8208 | tf_op jit(solution)/shard_map/reduce_scatter | solution.py:41
  186.0 22.5 %reduce-scatter.21.cloned.1.call-done = f32[16,128]{1,0:T(8,128)} async-done(((f32[64,128]{1,0:T(8,128)}), f32[16,128]{1,0:T(8,128)}) %reduce-scatter.21.cloned.1.call-update) | async-done | bytes 8208 | tf_op jit(solution)/shard_map/reduce_scatter | solution.py:41
  208.5 0.8 convert_bitcast_fusion.2
  209.5 1.3 bitcast_maximum_fusion.2
  210.8 0.7 fusion.74
  211.5 0.7 fusion.106
  212.4 0.8 fusion.1
  213.1 17.4 %reduce-scatter.27.cloned.1.call-done = f32[16,128]{1,0:T(8,128)} async-done(((f32[64,128]{1,0:T(8,128)}), f32[16,128]{1,0:T(8,128)}) %reduce-scatter.27.cloned.1.call-update) | async-done | bytes 8208 | tf_op jit(solution)/shard_map/reduce_scatter | solution.py:41
  230.5 0.8 multiply_convert_fusion.10
  231.3 5.2 %all_gather.14 = bf16[64,128]{1,0:T(8,128)(2,1)S(1)} all-gather(bf16[16,128]{1,0:T(8,128)(2,1)S(1)} %multiply_convert_fusion.10), channel_id=1, replica_groups=mesh['grp'=2,'tp'=4,'dp'=4] {'dp'}, dimensions={0}, use_global_device_ids=true | all-gather | bytes 20480 | tf_op jit(solution)/shard_map/all_gather | solution.py:81
  236.5 0.9 fusion.16
  237.4 0.6 pad_maximum_fusion.1
  238.0 0.6 pad_maximum_fusion.2
  238.6 0.7 multiply_add_fusion.1
  239.3 1.5 pad_maximum_fusion
  240.8 16.8 %reduce-scatter.29.cloned.1.call-done = f32[16,1024]{1,0:T(8,128)} async-done(((f32[64,1024]{1,0:T(8,128)}), f32[16,1024]{1,0:T(8,128)}) %reduce-scatter.29.cloned.1.call-update) | async-done | bytes 65552 | tf_op jit(solution)/shard_map/reduce_scatter | solution.py:85
  257.5 0.8 add_convert_fusion
  258.4 13.4 %all_gather.15 = bf16[64,1024]{1,0:T(8,128)(2,1)S(1)} all-gather(bf16[16,1024]{1,0:T(8,128)(2,1)S(1)} %add_convert_fusion), channel_id=1, replica_groups=mesh['grp'=2,'tp'=4,'dp'=4] {'tp'}, dimensions={0}, use_global_device_ids=true | all-gather | bytes 163840 | tf_op jit(solution)/shard_map/all_gather | solution.py:89
  271.7 0.7 copy.28
  (48 shorter events, 1.6 us)
Async XLA Ops:
  7.2 18.0 %copy-start.5 = (f32[2,1]{0,1:T(1,128)S(1)}, f32[2,1]{0,1:T(1,128)}, u32[]{:S(2)}) copy-start(f32[2,1]{0,1:T(1,128)} %param.19) | copy-start | bytes 28
  7.2 71.5 %copy-start.6 = (bf16[2,1,384,2]{2,3,1,0:T(2,128)(2,1)S(1)}, bf16[2,1,384,2]{2,3,1,0:T(2,128)(2,1)}, u32[]{:S(2)}) copy-start(bf16[2,1,384,2]{2,3,1,0:T(2,128)(2,1)} %param.18) | copy-start | bytes 9220
  7.2 71.6 %copy-start.4 = (f32[2,16,1]{1,2,0:T(1,128)S(1)}, f32[2,16,1]{1,2,0:T(1,128)}, u32[]{:S(2)}) copy-start(f32[2,16,1]{1,2,0:T(1,128)} %param.23) | copy-start | bytes 388
  7.2 73.0 %copy-start.3 = (f32[2,16,1,128]{3,2,1,0:T(1,128)S(1)}, f32[2,16,1,128]{3,2,1,0:T(1,128)}, u32[]{:S(2)}) copy-start(f32[2,16,1,128]{3,2,1,0:T(1,128)} %param.22) | copy-start | bytes 49156
  7.2 73.1 %copy-start = (f32[2,16,1,128,128]{4,3,2,1,0:T(8,128)S(1)}, f32[2,16,1,128,128]{4,3,2,1,0:T(8,128)}, u32[]{:S(2)}) copy-start(f32[2,16,1,128,128]{4,3,2,1,0:T(8,128)} %param.21) | copy-start | bytes 6291460
  7.2 98.5 %copy-start.2 = (bf16[2,128,1024]{2,1,0:T(8,128)(2,1)S(1)}, bf16[2,128,1024]{2,1,0:T(8,128)(2,1)}, u32[]{:S(2)}) copy-start(bf16[2,128,1024]{2,1,0:T(8,128)(2,1)} %param.20) | copy-start | bytes 1572868
  7.2 26.1 %reduce-scatter.13.cloned.1.call-start = ((), (), s32[]{:S(2)}) async-start(), calls=%async_computation.11 | async-start | bytes 40960 | tf_op jit(solution)/shard_map/reduce_scatter | solution.py:41
  8.1 98.5 %copy-start.1 = (bf16[64,1024]{1,0:T(8,128)(2,1)S(1)}, bf16[64,1024]{1,0:T(8,128)(2,1)}, u32[]{:S(2)}) copy-start(bf16[64,1024]{1,0:T(8,128)(2,1)} %param.12) | copy-start | bytes 393220
  10.0 45.3 %reduce-scatter.15.cloned.1.call-start = ((), (), s32[]{:S(2)}) async-start(), calls=%async_computation.12 | async-start | bytes 40960 | tf_op jit(solution)/shard_map/reduce_scatter | solution.py:41
  11.9 65.9 %reduce-scatter.11.cloned.1.call-start = ((), (), s32[]{:S(2)}) async-start(), calls=%async_computation.10 | async-start | bytes 40960 | tf_op jit(solution)/shard_map/reduce_scatter | solution.py:41
  13.8 85.9 %reduce-scatter.17.cloned.1.call-start = ((), (), s32[]{:S(2)}) async-start(), calls=%async_computation.13 | async-start | bytes 40960 | tf_op jit(solution)/shard_map/reduce_scatter | solution.py:41
  15.7 111.1 %reduce-scatter.19.cloned.1.call-start = ((), (), s32[]{:S(2)}) async-start(), calls=%async_computation.14 | async-start | bytes 327680 | tf_op jit(solution)/shard_map/reduce_scatter | solution.py:85
  106.6 57.5 %reduce-scatter.23.cloned.1.call-start = ((), (), s32[]{:S(2)}) async-start(), calls=%async_computation.16 | async-start | bytes 40960 | tf_op jit(solution)/shard_map/reduce_scatter | solution.py:41
  146.2 39.8 %reduce-scatter.25.cloned.1.call-start = ((), (), s32[]{:S(2)}) async-start(), calls=%async_computation.17 | async-start | bytes 40960 | tf_op jit(solution)/shard_map/reduce_scatter | solution.py:41
  148.1 60.5 %reduce-scatter.21.cloned.1.call-start = ((), (), s32[]{:S(2)}) async-start(), calls=%async_computation.15 | async-start | bytes 40960 | tf_op jit(solution)/shard_map/reduce_scatter | solution.py:41
  153.9 76.6 %reduce-scatter.27.cloned.1.call-start = ((), (), s32[]{:S(2)}) async-start(), calls=%async_computation.18 | async-start | bytes 40960 | tf_op jit(solution)/shard_map/reduce_scatter | solution.py:41
  154.7 102.9 %reduce-scatter.29.cloned.1.call-start = ((), (), s32[]{:S(2)}) async-start(), calls=%async_computation.19 | async-start | bytes 327680 | tf_op jit(solution)/shard_map/reduce_scatter | solution.py:85
Sparse Core Ops, SparseCore 0:
  11.0 22.2 reduce-scatter.12
  35.7 19.5 reduce-scatter.14
  58.3 19.5 reduce-scatter.10
  80.1 19.5 reduce-scatter.16
  106.7 19.9 reduce-scatter.18
  146.3 17.6 reduce-scatter.22
  166.5 19.5 reduce-scatter.24
  189.0 19.5 reduce-scatter.20
  210.9 19.5 reduce-scatter.26
  237.5 19.9 reduce-scatter.28
where the time goes:
time: 280 us; the launch traced here: 279 us
  waiting for transfers between devices  179 us (64%)
  blocking collectives  51.2 us (18%)
  matrix products  17.7 us (6%)
  between operations  14.3 us (5%)
  other arithmetic  14 us (5%)
    reduce_scatter x8, waiting for transfers between devices, shards(): summed = lax.psum_scatter(terms, 'dp', scatter_dimension=0, tiled=True)  142 us
    reduce_scatter x2, waiting for transfers between devices, shards(): mine = lax.psum_scatter(partial_mix, 'tp', scatter_dimension=0, tiled=True)  36.9 us
    all_gather x2, blocking collectives, shards(): x = lax.all_gather(updated, 'tp', axis=0, tiled=True)  26.7 us
    dot_general x8, matrix products, shards(): jnp.dot(scaled_in, weight[blk], preferred_element_type=jnp.float32)  14.2 us
    psum x2, blocking collectives, shards(): totals = lax.psum(squares, 'dp')  14 us
    all_gather x2, blocking collectives, shards(): lax.all_gather(gated, 'dp', axis=0, tiled=True)  10.4 us
  transfers between devices with their start and end apart: 10, of which 10 were waited for; matrix products, arithmetic and copies ran while one was open for 7% of the time, Pallas kernels for 0%

commit v1 on v0

--- a/solution.py
+++ b/solution.py
@@ -7,6 +7,18 @@
 DK = 128
 BLOCKS = 2
 EPS = 1e-06
+
+
+def doubled_up(value, axis, dim):
+    ways, here = (lax.axis_size(axis), lax.axis_index(axis))
+    grown, reach = (value, 1)
+    while reach < ways:
+        theirs = lax.ppermute(grown, axis, [(d, d ^ reach) for d in range(ways)])
+        mine_first = jnp.concatenate([grown, theirs], axis=dim)
+        theirs_first = jnp.concatenate([theirs, grown], axis=dim)
+        grown = jnp.where(here & reach == 0, mine_first, theirs_first)
+        reach = 2 * reach
+    return grown
 
 
 def shards(
@@ -86,7 +98,7 @@
         row_count = mine.shape[0]
         own_rows = lax.dynamic_slice_in_dim(xf, lax.axis_index("tp") * row_count, row_count, 0)
         updated = (own_rows + mine).astype(jnp.bfloat16)
-        x = lax.all_gather(updated, "tp", axis=0, tiled=True)
+        x = doubled_up(updated, "tp", 0)
         mems.append(new_mem)
         norms.append(new_norm)
         stabs.append(new_stab)

time: 280 us -> 269 us (0.961)
  blocking collectives: 51.2 us -> 24.4 us
  waiting for transfers between devices: 179 us -> 193 us
    all_gather x2 -> x0, blocking collectives: 26.7 us -> none  [shards(): x = lax.all_gather(updated, 'tp', axis=0, tiled=True)]
    ppermute x0 -> x4, waiting for transfers between devices: none -> 16 us  [doubled_up(): theirs = lax.ppermute(grown, axis, [(d, d ^ reach) for d in range(ways)])]
  transfers between devices with their start and end apart: 10 -> 14, of which waited for: 10 -> 14; matrix products, arithmetic and copies ran while one was open for 7% -> 9% of each run, Pallas kernels for 0% -> 0%
where the time goes in v1:
time: 269 us; the launch traced here: 268 us
  waiting for transfers between devices  193 us (72%)
  blocking collectives  24.4 us (9%)
  matrix products  17.8 us (7%)
  other arithmetic  14.8 us (6%)
  between operations  14.4 us (5%)
    reduce_scatter x8, waiting for transfers between devices, shards(): summed = lax.psum_scatter(terms, 'dp', scatter_dimension=0, tiled=True)  140 us
    reduce_scatter x2, waiting for transfers between devices, shards(): mine = lax.psum_scatter(partial_mix, 'tp', scatter_dimension=0, tiled=True)  36.7 us
    ppermute x4, waiting for transfers between devices, doubled_up(): theirs = lax.ppermute(grown, axis, [(d, d ^ reach) for d in range(ways)])  16 us
    dot_general x8, matrix products, shards(): jnp.dot(scaled_in, weight[blk], preferred_element_type=jnp.float32)  14.2 us
    psum x2, blocking collectives, shards(): totals = lax.psum(squares, 'dp')  14 us
    all_gather x2, blocking collectives, shards(): lax.all_gather(gated, 'dp', axis=0, tiled=True)  10.4 us
  transfers between devices with their start and end apart: 14, of which 14 were waited for; matrix products, arithmetic and copies ran while one was open for 9% of the time, Pallas kernels for 0%

profile of v1, /device:TPU:0, one launch (start us, length us, event | category | flops | bytes accessed | tf_op | source)
XLA Modules:
  0.0 268.3 jit_solution(12830532220922849592)
XLA Ops:
  7.3 0.9 fusion.117
  8.2 1.8 fusion.32
  10.1 1.8 fusion.30
  11.9 1.8 fusion.34
  13.8 1.8 fusion.28
  15.7 1.0 multiply_reduce_fusion.1
  16.8 8.4 %psum.14 = f32[64]{0:T(128)S(1)} all-reduce(f32[64]{0:T(128)S(1)} %multiply_reduce_fusion.1), channel_id=1, replica_groups=mesh['grp'=2,'tp'=4,'dp'=4] {'dp'}, use_global_device_ids=true, to_apply=%region_1.0 | all-reduce | flops 64 | bytes 512 | tf_op jit(solution)/shard_map/psum | solution.py:52
  25.8 7.5 %reduce-scatter.13.cloned.1.call-done = f32[16,128]{1,0:T(8,128)} async-done(((f32[64,128]{1,0:T(8,128)}), f32[16,128]{1,0:T(8,128)}) %reduce-scatter.13.cloned.1.call-update) | async-done | bytes 8208 | tf_op jit(solution)/shard_map/reduce_scatter | solution.py:53
  33.3 22.0 %reduce-scatter.15.cloned.1.call-done = f32[16,128]{1,0:T(8,128)} async-done(((f32[64,128]{1,0:T(8,128)}), f32[16,128]{1,0:T(8,128)}) %reduce-scatter.15.cloned.1.call-update) | async-done | bytes 8208 | tf_op jit(solution)/shard_map/reduce_scatter | solution.py:53
  55.3 22.5 %reduce-scatter.11.cloned.1.call-done = f32[16,128]{1,0:T(8,128)} async-done(((f32[64,128]{1,0:T(8,128)}), f32[16,128]{1,0:T(8,128)}) %reduce-scatter.11.cloned.1.call-update) | async-done | bytes 8208 | tf_op jit(solution)/shard_map/reduce_scatter | solution.py:53
  77.8 0.8 convert_bitcast_fusion.3
  78.8 0.7 fusion.71
  79.4 0.7 fusion.109
  80.4 0.8 fusion.4
  81.1 18.6 %reduce-scatter.17.cloned.1.call-done = f32[16,128]{1,0:T(8,128)} async-done(((f32[64,128]{1,0:T(8,128)}), f32[16,128]{1,0:T(8,128)}) %reduce-scatter.17.cloned.1.call-update) | async-done | bytes 8208 | tf_op jit(solution)/shard_map/reduce_scatter | solution.py:53
  99.7 0.8 multiply_convert_fusion.11
  100.5 5.2 %all_gather.6 = bf16[64,128]{1,0:T(8,128)(2,1)S(1)} all-gather(bf16[16,128]{1,0:T(8,128)(2,1)S(1)} %multiply_convert_fusion.11), channel_id=1, replica_groups=mesh['grp'=2,'tp'=4,'dp'=4] {'dp'}, dimensions={0}, use_global_device_ids=true | all-gather | bytes 20480 | tf_op jit(solution)/shard_map/all_gather | solution.py:93
  105.7 0.9 fusion.26
  106.7 20.1 %reduce-scatter.19.cloned.1.call-done = f32[16,1024]{1,0:T(8,128)} async-done(((f32[64,1024]{1,0:T(8,128)}), f32[16,1024]{1,0:T(8,128)}) %reduce-scatter.19.cloned.1.call-update) | async-done | bytes 65552 | tf_op jit(solution)/shard_map/reduce_scatter | solution.py:97
  126.8 0.8 add_convert_fusion.1
  127.7 4.0 %collective-permute-done = bf16[16,1024]{1,0:T(8,128)(2,1)S(1)} collective-permute-done((bf16[16,1024]{1,0:T(8,128)(2,1)S(1)}, bf16[16,1024]{1,0:T(8,128)(2,1)S(1)}, u32[]{:S(2)}, u32[]{:S(2)}) %collective-permute-start) | collective-permute-done | bytes 32800 | tf_op jit(solution)/shard_map/ppermute | solution.py:16
  131.7 0.9 collective-permute-start.1
  132.6 4.7 %collective-permute-done.1 = bf16[32,1024]{1,0:T(8,128)(2,1)S(1)} collective-permute-done((bf16[32,1024]{1,0:T(8,128)(2,1)S(1)}, bf16[32,1024]{1,0:T(8,128)(2,1)S(1)}, u32[]{:S(2)}, u32[]{:S(2)}) %collective-permute-start.1) | collective-permute-done | bytes 65568 | tf_op jit(solution)/shard_map/ppermute | solution.py:16
  137.3 1.7 fusion.22
  139.1 1.7 fusion.20
  141.0 1.8 fusion.24
  142.9 5.7 %psum.15 = f32[64]{0:T(128)S(1)} all-reduce(f32[64]{0:T(128)S(1)} %multiply_reduce_fusion), channel_id=1, replica_groups=mesh['grp'=2,'tp'=4,'dp'=4] {'dp'}, use_global_device_ids=true, to_apply=%region_9.10 | all-reduce | flops 64 | bytes 512 | tf_op jit(solution)/shard_map/psum | solution.py:52
  148.6 1.7 fusion.18
  150.5 6.4 %reduce-scatter.23.cloned.1.call-done = f32[16,128]{1,0:T(8,128)} async-done(((f32[64,128]{1,0:T(8,128)}), f32[16,128]{1,0:T(8,128)}) %reduce-scatter.23.cloned.1.call-update) | async-done | bytes 8208 | tf_op jit(solution)/shard_map/reduce_scatter | solution.py:53
  156.9 22.0 %reduce-scatter.25.cloned.1.call-done = f32[16,128]{1,0:T(8,128)} async-done(((f32[64,128]{1,0:T(8,128)}), f32[16,128]{1,0:T(8,128)}) %reduce-scatter.25.cloned.1.call-update) | async-done | bytes 8208 | tf_op jit(solution)/shard_map/reduce_scatter | solution.py:53
  178.9 22.6 %reduce-scatter.21.cloned.1.call-done = f32[16,128]{1,0:T(8,128)} async-done(((f32[64,128]{1,0:T(8,128)}), f32[16,128]{1,0:T(8,128)}) %reduce-scatter.21.cloned.1.call-update) | async-done | bytes 8208 | tf_op jit(solution)/shard_map/reduce_scatter | solution.py:53
  201.5 0.8 convert_bitcast_fusion.2
  202.4 0.7 fusion.75
  203.1 0.7 fusion.107
  204.0 0.8 fusion.1
  204.7 18.7 %reduce-scatter.27.cloned.1.call-done = f32[16,128]{1,0:T(8,128)} async-done(((f32[64,128]{1,0:T(8,128)}), f32[16,128]{1,0:T(8,128)}) %reduce-scatter.27.cloned.1.call-update) | async-done | bytes 8208 | tf_op jit(solution)/shard_map/reduce_scatter | solution.py:53
  223.5 0.8 multiply_convert_fusion.6
  224.2 5.2 %all_gather.7 = bf16[64,128]{1,0:T(8,128)(2,1)S(1)} all-gather(bf16[16,128]{1,0:T(8,128)(2,1)S(1)} %multiply_convert_fusion.6), channel_id=1, replica_groups=mesh['grp'=2,'tp'=4,'dp'=4] {'dp'}, dimensions={0}, use_global_device_ids=true | all-gather | bytes 20480 | tf_op jit(solution)/shard_map/all_gather | solution.py:93
  229.4 0.9 fusion.16
  230.3 0.8 multiply_add_fusion.1
  231.1 1.5 pad_maximum_fusion
  232.6 1.3 bitcast_maximum_fusion.2
  233.9 16.6 %reduce-scatter.29.cloned.1.call-done = f32[16,1024]{1,0:T(8,128)} async-done(((f32[64,1024]{1,0:T(8,128)}), f32[16,1024]{1,0:T(8,128)}) %reduce-scatter.29.cloned.1.call-update) | async-done | bytes 65552 | tf_op jit(solution)/shard_map/reduce_scatter | solution.py:97
  250.5 0.8 add_convert_fusion
  252.0 3.4 %collective-permute-done.2 = bf16[16,1024]{1,0:T(8,128)(2,1)S(1)} collective-permute-done((bf16[16,1024]{1,0:T(8,128)(2,1)S(1)}, bf16[16,1024]{1,0:T(8,128)(2,1)S(1)}, u32[]{:S(2)}, u32[]{:S(2)}) %collective-permute-start.2) | collective-permute-done | bytes 32800 | tf_op jit(solution)/shard_map/ppermute | solution.py:16
  255.5 0.9 collective-permute-start.3
  257.0 3.8 %collective-permute-done.3 = bf16[32,1024]{1,0:T(8,128)(2,1)S(1)} collective-permute-done((bf16[32,1024]{1,0:T(8,128)(2,1)S(1)}, bf16[32,1024]{1,0:T(8,128)(2,1)S(1)}, u32[]{:S(2)}, u32[]{:S(2)}) %collective-permute-start.3) | collective-permute-done | bytes 65568 | tf_op jit(solution)/shard_map/ppermute | solution.py:16
  260.8 0.7 maximum_select_fusion.1
  (56 shorter events, 3.5 us)
Async XLA Ops:
  7.2 18.0 %copy-start.5 = (f32[2,1]{0,1:T(1,128)S(1)}, f32[2,1]{0,1:T(1,128)}, u32[]{:S(2)}) copy-start(f32[2,1]{0,1:T(1,128)} %param.19) | copy-start | bytes 28
  7.2 71.5 %copy-start.6 = (bf16[2,1,384,2]{2,3,1,0:T(2,128)(2,1)S(1)}, bf16[2,1,384,2]{2,3,1,0:T(2,128)(2,1)}, u32[]{:S(2)}) copy-start(bf16[2,1,384,2]{2,3,1,0:T(2,128)(2,1)} %param.18) | copy-start | bytes 9220
  7.2 71.6 %copy-start.4 = (f32[2,16,1]{1,2,0:T(1,128)S(1)}, f32[2,16,1]{1,2,0:T(1,128)}, u32[]{:S(2)}) copy-start(f32[2,16,1]{1,2,0:T(1,128)} %param.23) | copy-start | bytes 388
  7.2 73.0 %copy-start.3 = (f32[2,16,1,128]{3,2,1,0:T(1,128)S(1)}, f32[2,16,1,128]{3,2,1,0:T(1,128)}, u32[]{:S(2)}) copy-start(f32[2,16,1,128]{3,2,1,0:T(1,128)} %param.22) | copy-start | bytes 49156
  7.2 73.1 %copy-start = (f32[2,16,1,128,128]{4,3,2,1,0:T(8,128)S(1)}, f32[2,16,1,128,128]{4,3,2,1,0:T(8,128)}, u32[]{:S(2)}) copy-start(f32[2,16,1,128,128]{4,3,2,1,0:T(8,128)} %param.21) | copy-start | bytes 6291460
  7.2 98.5 %copy-start.2 = (bf16[2,128,1024]{2,1,0:T(8,128)(2,1)S(1)}, bf16[2,128,1024]{2,1,0:T(8,128)(2,1)}, u32[]{:S(2)}) copy-start(bf16[2,128,1024]{2,1,0:T(8,128)(2,1)} %param.20) | copy-start | bytes 1572868
  7.2 26.1 %reduce-scatter.13.cloned.1.call-start = ((), (), s32[]{:S(2)}) async-start(), calls=%async_computation.11 | async-start | bytes 40960 | tf_op jit(solution)/shard_map/reduce_scatter | solution.py:53
  8.1 98.5 %copy-start.1 = (bf16[64,1024]{1,0:T(8,128)(2,1)S(1)}, bf16[64,1024]{1,0:T(8,128)(2,1)}, u32[]{:S(2)}) copy-start(bf16[64,1024]{1,0:T(8,128)(2,1)} %param.12) | copy-start | bytes 393220
  10.0 45.3 %reduce-scatter.15.cloned.1.call-start = ((), (), s32[]{:S(2)}) async-start(), calls=%async_computation.12 | async-start | bytes 40960 | tf_op jit(solution)/shard_map/reduce_scatter | solution.py:53
  11.9 65.9 %reduce-scatter.11.cloned.1.call-start = ((), (), s32[]{:S(2)}) async-start(), calls=%async_computation.10 | async-start | bytes 40960 | tf_op jit(solution)/shard_map/reduce_scatter | solution.py:53
  13.8 85.9 %reduce-scatter.17.cloned.1.call-start = ((), (), s32[]{:S(2)}) async-start(), calls=%async_computation.13 | async-start | bytes 40960 | tf_op jit(solution)/shard_map/reduce_scatter | solution.py:53
  15.7 111.1 %reduce-scatter.19.cloned.1.call-start = ((), (), s32[]{:S(2)}) async-start(), calls=%async_computation.14 | async-start | bytes 327680 | tf_op jit(solution)/shard_map/reduce_scatter | solution.py:97
  106.6 50.3 %reduce-scatter.23.cloned.1.call-start = ((), (), s32[]{:S(2)}) async-start(), calls=%async_computation.16 | async-start | bytes 40960 | tf_op jit(solution)/shard_map/reduce_scatter | solution.py:53
  127.6 4.1 %collective-permute-start = (bf16[16,1024]{1,0:T(8,128)(2,1)S(1)}, bf16[16,1024]{1,0:T(8,128)(2,1)S(1)}, u32[]{:S(2)}, u32[]{:S(2)}) collective-permute-start(bf16[16,1024]{1,0:T(8,128)(2,1)S(1)} %add_convert_fusion.1), channel_id=1, source_target_pairs={{0,4},{4,0},{8,12},{12,8},{1,5},{5,1},{9,13},{13,9},{2,6},{6,2},{1... | collective-permute-start | bytes 98312 | tf_op jit(solution)/shard_map/ppermute | solution.py:16
  131.7 5.6 %collective-permute-start.1 = (bf16[32,1024]{1,0:T(8,128)(2,1)S(1)}, bf16[32,1024]{1,0:T(8,128)(2,1)S(1)}, u32[]{:S(2)}, u32[]{:S(2)}) collective-permute-start(bf16[32,1024]{1,0:T(8,128)(2,1)S(1)} %maximum_select_fusion.2), channel_id=1, source_target_pairs={{0,8},{4,12},{8,0},{12,4},{1,9},{5,13},{9,1},{13,5},{2,10},{6,14},... | collective-permute-start | bytes 196616 | tf_op jit(solution)/shard_map/ppermute | solution.py:16
  139.1 39.8 %reduce-scatter.25.cloned.1.call-start = ((), (), s32[]{:S(2)}) async-start(), calls=%async_computation.17 | async-start | bytes 40960 | tf_op jit(solution)/shard_map/reduce_scatter | solution.py:53
  140.9 60.6 %reduce-scatter.21.cloned.1.call-start = ((), (), s32[]{:S(2)}) async-start(), calls=%async_computation.15 | async-start | bytes 40960 | tf_op jit(solution)/shard_map/reduce_scatter | solution.py:53
  148.5 74.9 %reduce-scatter.27.cloned.1.call-start = ((), (), s32[]{:S(2)}) async-start(), calls=%async_computation.18 | async-start | bytes 40960 | tf_op jit(solution)/shard_map/reduce_scatter | solution.py:53
  150.4 100.1 %reduce-scatter.29.cloned.1.call-start = ((), (), s32[]{:S(2)}) async-start(), calls=%async_computation.19 | async-start | bytes 327680 | tf_op jit(solution)/shard_map/reduce_scatter | solution.py:97
  251.4 4.1 %collective-permute-start.2 = (bf16[16,1024]{1,0:T(8,128)(2,1)S(1)}, bf16[16,1024]{1,0:T(8,128)(2,1)S(1)}, u32[]{:S(2)}, u32[]{:S(2)}) collective-permute-start(bf16[16,1024]{1,0:T(8,128)(2,1)S(1)} %add_convert_fusion), channel_id=1, source_target_pairs={{0,4},{4,0},{8,12},{12,8},{1,5},{5,1},{9,13},{13,9},{2,6},{6,2},{1... | collective-permute-start | bytes 98312 | tf_op jit(solution)/shard_map/ppermute | solution.py:16
  255.5 5.3 %collective-permute-start.3 = (bf16[32,1024]{1,0:T(8,128)(2,1)S(1)}, bf16[32,1024]{1,0:T(8,128)(2,1)S(1)}, u32[]{:S(2)}, u32[]{:S(2)}) collective-permute-start(bf16[32,1024]{1,0:T(8,128)(2,1)S(1)} %maximum_select_fusion.3), channel_id=1, source_target_pairs={{0,8},{4,12},{8,0},{12,4},{1,9},{5,13},{9,1},{13,5},{2,10},{6,14},... | collective-permute-start | bytes 196616 | tf_op jit(solution)/shard_map/ppermute | solution.py:16
Sparse Core Ops, SparseCore 0:
  11.0 22.2 reduce-scatter.12
  35.7 19.5 reduce-scatter.14
  58.3 19.5 reduce-scatter.10
  80.1 19.5 reduce-scatter.16
  106.7 19.9 reduce-scatter.18
  139.2 17.6 reduce-scatter.22
  159.3 19.5 reduce-scatter.24
  181.9 19.5 reduce-scatter.20
  203.9 19.5 reduce-scatter.26
  230.5 19.9 reduce-scatter.28
